TPU v7x, 32 devices: a whole 2x2x4 slice. The times are simulated.
32 devices in a mesh: sp: 16 (over z, y, core), tp: 2 (over x).
Axes of the slice: x: 2, y: 2, z: 4, core: 2. Of those that a mesh axis runs over, the one named last changes fastest.
Arguments:
- tokens: bfloat16 [12288, 2048], P(('sp', 'tp')), may hold values from -6 to 6
- norm_gain: float32 [2048], replicated, may hold values from 0.1 to 1.9
- query_weight: bfloat16 [2048, 512], P(None, 'tp'), may hold values from -4 to 4
- key_weight: bfloat16 [2048, 256], P(None, 'tp'), may hold values from -4 to 4
- value_weight: bfloat16 [2048, 256], P(None, 'tp'), may hold values from -1 to 1
- sink_logit: float32 [8], P('tp'), may hold values from 2 to 6
- conv_gate_weight: bfloat16 [2048, 512], P(None, 'tp'), may hold values from -0.125 to 0.125
- conv_pre_weight: bfloat16 [2048, 512], P(None, 'tp'), may hold values from -0.125 to 0.125
- conv_input_weight: bfloat16 [2048, 512], P(None, 'tp'), may hold values from -0.125 to 0.125
- conv_taps: float32 [3, 512], P(None, 'tp'), may hold values from -3.5 to 3.5
- out_weight: bfloat16 [1024, 2048], replicated, may hold values from -0.1875 to 0.1875
Outputs:
- mixed: bfloat16 [12288, 2048], P(('sp', 'tp'))
All inputs are finite; a program needn't handle non-finite values.
Results may differ from a plain program's by a relative error of at most 0.009.
Values may be sent and summed in bfloat16 or wider, within the bound.
A program may use at most 64 MiB of HBM per device.

v0:
```python
import jax
import jax.numpy as jnp
from jax import lax
from jax.sharding import PartitionSpec as P

QH = 8
KVH = 4
HEAD_SIZE = 64
WIN = 128


def extended(block, sides, width):
    for axis, dim in sides:
        count = lax.axis_size(axis)
        forward = [(i, i + 1) for i in range(count - 1)]
        backward = [(target, source) for source, target in forward]
        low = lax.ppermute(
            lax.slice_in_dim(block, block.shape[dim] - width, None, axis=dim), axis, forward
        )
        high = lax.ppermute(lax.slice_in_dim(block, 0, width, axis=dim), axis, backward)
        block = jnp.concatenate([low, block, high], axis=dim)
    return block


def attend_local(query_block_tile, key_block_tile, value_block_tile, start, sinks, total):
    count = query_block_tile.shape[0]
    span = key_block_tile.shape[0]
    score_matrix = jnp.einsum(
        "yxpz,ixz->xpyi", query_block_tile, key_block_tile, preferred_element_type=jnp.float32
    ) * HEAD_SIZE ** (-0.5)
    query_pos = start + jnp.arange(count, dtype=jnp.int32)
    key_pos = start - WIN + jnp.arange(span, dtype=jnp.int32)
    valid = (
        (jnp.abs(query_pos[:, None] - key_pos[None, :]) <= WIN)
        & (key_pos[None, :] >= 0)
        & (key_pos[None, :] < total)
    )
    score_matrix = jnp.where(valid[None, None], score_matrix, -jnp.inf)
    sink_col = sinks[:, :, None, None]
    top = jnp.maximum(jnp.max(score_matrix, axis=-1, keepdims=True), sink_col)
    expo = jnp.exp(score_matrix - top)
    denom = jnp.sum(expo, axis=-1, keepdims=True) + jnp.exp(sink_col - top)
    weight_lower_precision = (expo / denom).astype(jnp.bfloat16)
    final_output = jnp.einsum(
        "bhcv,vbn->cbhn",
        weight_lower_precision,
        value_block_tile,
        preferred_element_type=jnp.float32,
    )
    return final_output.reshape(count, -1).astype(jnp.bfloat16)


def short_conv(conv_pad, conv_taps, conv_gate):
    count = conv_gate.shape[0]
    conv_f = conv_pad.astype(jnp.float32)
    convolved = (
        conv_taps[0] * conv_f[0:count]
        + conv_taps[1] * conv_f[1 : count + 1]
        + conv_taps[2] * conv_f[2 : count + 2]
    )
    return (conv_gate.astype(jnp.float32) * convolved).astype(jnp.bfloat16)


def body(
    tokens,
    norm_gain,
    query_weight,
    key_weight,
    value_weight,
    sink_logit,
    conv_gate_weight,
    conv_pre_weight,
    conv_input_weight,
    conv_taps,
    out_weight,
):
    tokens_f = tokens.astype(jnp.float32)
    normed = (
        tokens_f
        * lax.rsqrt(jnp.mean(tokens_f * tokens_f, axis=-1, keepdims=True) + 1e-06)
        * norm_gain
    ).astype(jnp.bfloat16)
    all_weight = jnp.concatenate(
        [
            query_weight,
            key_weight,
            value_weight,
            conv_gate_weight,
            conv_pre_weight,
            conv_input_weight,
        ],
        axis=1,
    )
    projected = jnp.dot(
        lax.all_gather(normed, "tp", axis=0, tiled=True),
        all_weight,
        preferred_element_type=jnp.float32,
    ).astype(jnp.bfloat16)
    query_width = query_weight.shape[1]
    kv_width = key_weight.shape[1]
    conv_width = conv_gate_weight.shape[1]
    edge_key = query_width + kv_width
    edge_value = edge_key + kv_width
    edge_gate = edge_value + conv_width
    edge_pre = edge_gate + conv_width
    queries = projected[:, :query_width]
    key_rows = projected[:, query_width:edge_key]
    value_rows = projected[:, edge_key:edge_value]
    conv_gate = projected[:, edge_value:edge_gate]
    conv_pre = projected[:, edge_gate:edge_pre]
    conv_input = projected[:, edge_pre:]
    product = (conv_pre.astype(jnp.float32) * conv_input.astype(jnp.float32)).astype(jnp.bfloat16)
    count = projected.shape[0]
    offset = lax.axis_index("sp") * count
    total = count * lax.axis_size("sp")
    padded = extended(jnp.concatenate([key_rows, value_rows, product], 1), (("sp", 0),), WIN)
    key_pad = padded[:, :kv_width]
    value_pad = padded[:, kv_width : 2 * kv_width]
    conv_pad = padded[WIN - 1 : WIN + count + 1, 2 * kv_width :]
    groups = kv_width // HEAD_SIZE
    ratio = QH // KVH
    query_block_tile = queries.reshape(count, groups, ratio, HEAD_SIZE)
    key_block_tile = key_pad.reshape(-1, groups, HEAD_SIZE)
    value_block_tile = value_pad.reshape(-1, groups, HEAD_SIZE)
    sinks = sink_logit.reshape(groups, ratio)
    conv_out = short_conv(conv_pad, conv_taps, conv_gate)
    attended = attend_local(
        query_block_tile, key_block_tile, value_block_tile, offset, sinks, total
    )
    attn_rows, conv_rows = (
        lax.all_to_all(attended, "tp", split_axis=0, concat_axis=1, tiled=True),
        lax.all_to_all(conv_out, "tp", split_axis=0, concat_axis=1, tiled=True),
    )
    joined = jnp.concatenate([attn_rows, conv_rows], axis=1)
    return jnp.dot(joined, out_weight, preferred_element_type=jnp.float32).astype(jnp.bfloat16)


def solution(mesh):
    placed = (
        P(("sp", "tp"), None),
        P(),
        P(None, "tp"),
        P(None, "tp"),
        P(None, "tp"),
        P("tp"),
        P(None, "tp"),
        P(None, "tp"),
        P(None, "tp"),
        P(None, "tp"),
        P(),
    )
    return jax.shard_map(
        body, mesh=mesh, in_specs=placed, out_specs=P(("sp", "tp"), None), check_vma=False
    )
```

profile of v0, /device:TPU:8, one launch (start us, length us, event | category | flops | bytes accessed | tf_op | source)
XLA Modules:
  0.0 116.7 jit_solution(4361045955193434557)
XLA Ops:
  6.5 1.9 %fusion.3 = f32[384]{0:T(512)S(1)} fusion(bf16[384,2048]{1,0:T(8,128)(2,1)} %param.11), kind=kLoop, calls=%fused_computation.9 | loop fusion | flops 2358912 | bytes 1574400 | tf_op jit(solution)/shard_map/reduce_sum | solution.py:80
  8.5 3.1 %fusion.5 = bf16[384,2048]{1,0:T(8,128)(2,1)} fusion(bf16[384,2048]{1,0:T(8,128)(2,1)} %param.11, f32[2048]{0:T(1024)} %param.12, f32[384]{0:T(512)S(1)} %add_rsqrt_fusion), kind=kLoop, calls=%fused_computation.11 | loop fusion | flops 3145728 | bytes 3155456 | tf_op jit(solution)/shard_map/convert_element_type | solution.py:82
  11.8 1.2 %constant_dynamic-update-slice_fusion.4 = bf16[2048,1280]{1,0:T(8,128)(2,1)S(1)} fusion(bf16[2048,1280]{1,0:T(8,128)(2,1)S(1)} %constant_dynamic-update-slice_fusion.5, bf16[2048,128]{1,0:T(8,128)(2,1)} %param.14), kind=kLoop, calls=%fused_computation.41 | loop fusion | bytes 1048576
  13.0 1.2 %constant_dynamic-update-slice_fusion.3 = bf16[2048,1280]{1,0:T(8,128)(2,1)S(1)} fusion(bf16[2048,1280]{1,0:T(8,128)(2,1)S(1)} %constant_dynamic-update-slice_fusion.4, bf16[2048,128]{1,0:T(8,128)(2,1)} %param.15), kind=kLoop, calls=%fused_computation.40 | loop fusion | bytes 1048576
  14.5 2.3 %copy-done.4 = bf16[2048,1280]{1,0:T(8,128)(2,1)} copy-done((bf16[2048,1280]{1,0:T(8,128)(2,1)}, bf16[2048,1280]{1,0:T(8,128)(2,1)S(1)}, u32[]{:S(2)}) %copy-start.4) | copy-done | bytes 5242904
  16.8 1.4 %fusion.7 = pred[768,1024]{0,1:T(8,128)(4,1)S(1)} fusion(s32[1024]{0:T(1024)S(1)} %iota_add_fusion, s32[768]{0:T(1024)S(1)} %iota_add_fusion.1, pred[1024]{0:T(1024)(128)(4,1)S(1)} %get-tuple-element.16, pred[1024]{0:T(1024)(128)(4,1)S(1)} %get-tuple-element.17), kind=kLoop, calls=%fused_computation.14 | loop fusion | flops 3932160 | bytes 795648 | tf_op jit(solution)/shard_map/and | solution.py:34
  18.1 39.7 %all-gather.2.cloned.1.call-done = bf16[768,2048]{1,0:T(8,128)(2,1)} async-done(((bf16[384,2048]{1,0:T(8,128)(2,1)}), bf16[768,2048]{1,0:T(8,128)(2,1)}) %all-gather.2.cloned.1.call-update) | async-done | bytes 3145744 | tf_op jit(solution)/shard_map/all_gather | solution.py:95
  57.8 7.7 %convolution_convert_fusion = bf16[768,1280]{1,0:T(8,128)(2,1)S(1)} fusion(bf16[768,2048]{1,0:T(8,128)(2,1)} %all-gather.2.cloned.1.call-done, bf16[2048,1280]{1,0:T(8,128)(2,1)} %copy-done.4), kind=kOutput, calls=%fused_computation.8 | convolution fusion | flops 4027514880 | bytes 10354688 | tf_op jit(solution)/shard_map/dot_general | solution.py:94
  65.6 0.8 fusion.23
  66.4 0.7 pad_maximum_fusion.6
  67.1 2.6 %collective-permute-start.1 = (bf16[128,512]{1,0:T(8,128)(2,1)}, bf16[128,512]{1,0:T(8,128)(2,1)}, u32[]{:S(2)}, u32[]{:S(2)}) collective-permute-start(bf16[128,512]{1,0:T(8,128)(2,1)} %get-tuple-element.10), channel_id=1, source_target_pairs={{2,0},{4,2},{6,4},{8,6},{10,8},{12,10},{14,12},{16,14},{18,16},{20... | collective-permute-start | bytes 393224 | tf_op jit(solution)/shard_map/ppermute | solution.py:20
  69.7 1.9 %collective-permute-start = (bf16[128,512]{1,0:T(8,128)(2,1)}, bf16[128,512]{1,0:T(8,128)(2,1)}, u32[]{:S(2)}, u32[]{:S(2)}) collective-permute-start(bf16[128,512]{1,0:T(8,128)(2,1)} %get-tuple-element.9), channel_id=1, source_target_pairs={{0,2},{2,4},{4,6},{6,8},{8,10},{10,12},{12,14},{14,16},{16,18},{18... | collective-permute-start | bytes 393224 | tf_op jit(solution)/shard_map/ppermute | solution.py:17
  71.7 1.9 %copy.18 = bf16[768,256]{0,1:T(8,128)(2,1)} copy(bf16[768,256]{1,0:T(8,128)(2,1)} %get-tuple-element.5) | data formatting | bytes 786432 | tf_op jit(solution)/shard_map/slice | solution.py:106
  73.6 3.6 %collective-permute-done = bf16[128,512]{1,0:T(8,128)(2,1)} collective-permute-done((bf16[128,512]{1,0:T(8,128)(2,1)}, bf16[128,512]{1,0:T(8,128)(2,1)}, u32[]{:S(2)}, u32[]{:S(2)}) %collective-permute-start) | collective-permute-done | bytes 131104 | tf_op jit(solution)/shard_map/ppermute | solution.py:17
  77.2 0.8 fusion.17
  78.0 1.0 fusion.12
  79.1 1.9 %copy.21 = bf16[2,384,256]{1,2,0:T(8,128)(2,1)} copy(bf16[2,384,256]{2,1,0:T(8,128)(2,1)} %bitcast.46) | data formatting | bytes 786432 | tf_op jit(solution)/shard_map/all_to_all | solution.py:132
  81.0 3.6 %all-to-all-start.1 = ((bf16[2,384,256]{1,2,0:T(8,128)(2,1)}), bf16[2,384,256]{1,2,0:T(8,128)(2,1)S(1)}, u32[]{:S(2)}, u32[]{:S(2)}) async-start(bf16[2,384,256]{1,2,0:T(8,128)(2,1)} %copy.21), calls=%async_computation.1 | async-start | bytes 786432 | tf_op jit(solution)/shard_map/all_to_all | solution.py:132
  84.6 0.8 pad_maximum_fusion.3
  85.8 3.2 %fusion.1 = (f32[2,2,768]{2,1,0:T(2,128)S(1)}, f32[2,1024,768,2]{2,1,3,0:T(8,128)S(1)}) fusion(pred[768,1024]{0,1:T(8,128)(4,1)S(1)} %fusion.7, bf16[1024,2,64,1]{0,2,3,1:T(8,128)(2,1)S(1)} %bitcast.51, bf16[768,2,2,64]{0,3,2,1:T(8,128)(2,1)} %bitcast.48), kind=kOutput, calls=%fused_computation.4 | convolution fusion | flops 412087296 | bytes 14036992 | tf_op jit(solution)/shard_map/yxpz,ixz->xpyi/dot_general | solution.py:28
  89.1 2.7 %fusion = f32[2,2,768]{2,1,0:T(2,128)S(1)} fusion(f32[2,1024,768,2]{2,1,3,0:T(8,128)S(1)} %get-tuple-element.15, f32[2,2,768]{2,1,0:T(2,128)S(1)} %broadcast_maximum_fusion, pred[768,1024]{0,1:T(8,128)(4,1)S(1)} %fusion.7), kind=kLoop, calls=%fused_computation.3 | loop fusion | flops 12579840 | bytes 13393920 | tf_op jit(solution)/shard_map/reduce_sum | solution.py:42
  91.9 3.9 %fusion.9 = bf16[768,2,2,64]{0,3,2,1:T(8,128)(2,1)S(1)} fusion(bf16[1024,2,64,1]{0,2,3,1:T(8,128)(2,1)S(1)} %bitcast.50, f32[2,1024,768,2]{2,1,3,0:T(8,128)S(1)} %get-tuple-element.15, f32[2,2,768]{2,1,0:T(2,128)S(1)} %exponential_add_fusion, f32[2,2,768]{2,1,0:T(2,128)S(1)} %broadcast_maximum_fusion, pred[768,1024]{0,1:T(8,128)(4,1)S(1)} %fusion.7), kind=kOutput, calls=%fused_computation.17 | convolution fusion | flops 418578432 | bytes 14049280 | tf_op jit(solution)/shard_map/bhcv,vbn->cbhn/dot_general | solution.py:44
  96.0 8.8 %all_to_all.35 = bf16[2,384,256]{1,2,0:T(8,128)(2,1)S(1)} all-to-all(bf16[2,384,256]{1,2,0:T(8,128)(2,1)S(1)} %copy.20), channel_id=1, replica_groups=mesh['sp'=16,'tp'=2] {'tp'}, dimensions={0} | all-to-all | bytes 786432 | tf_op jit(solution)/shard_map/all_to_all | solution.py:131
  104.7 5.2 %convolution_convert_fusion.1 = bf16[384,2048]{1,0:T(8,128)(2,1)} fusion(bf16[1024,2048]{1,0:T(8,128)(2,1)} %param.21, bf16[384,512]{0,1:T(8,128)(2,1)S(1)} %bitcast.47, bf16[384,512]{0,1:T(8,128)(2,1)S(1)} %bitcast.49), kind=kOutput, calls=%fused_computation.15 | convolution fusion | flops 1612972032 | bytes 6553600 | tf_op jit(solution)/shard_map/dot_general | solution.py:135
  (34 shorter events, 1.1 us)
Async XLA Ops:
  6.5 5.1 %copy-start.6 = (f32[4]{0:T(128)S(1)}, f32[4]{0:T(128)}, u32[]{:S(2)}) copy-start(f32[4]{0:T(128)} %param.16) | copy-start | bytes 52
  6.5 5.2 %copy-start = (bf16[2048,256]{1,0:T(8,128)(2,1)S(1)}, bf16[2048,256]{1,0:T(8,128)(2,1)}, u32[]{:S(2)}) copy-start(bf16[2048,256]{1,0:T(8,128)(2,1)} %param.13) | copy-start | bytes 3145732
  6.5 7.7 %copy-start.1 = (bf16[2048,256]{1,0:T(8,128)(2,1)S(1)}, bf16[2048,256]{1,0:T(8,128)(2,1)}, u32[]{:S(2)}) copy-start(bf16[2048,256]{1,0:T(8,128)(2,1)} %param.17) | copy-start | bytes 3145732
  6.5 51.3 %all-gather.2.cloned.1.call-start = ((), (), s32[]{:S(2)}) async-start(), calls=%async_computation.2 | async-start | bytes 4718592 | tf_op jit(solution)/shard_map/all_gather | solution.py:95
  8.5 5.8 %copy-start.2 = (bf16[2048,256]{1,0:T(8,128)(2,1)S(1)}, bf16[2048,256]{1,0:T(8,128)(2,1)}, u32[]{:S(2)}) copy-start(bf16[2048,256]{1,0:T(8,128)(2,1)} %param.18) | copy-start | bytes 3145732
  11.7 2.7 %copy-start.3 = (bf16[2048,256]{1,0:T(8,128)(2,1)S(1)}, bf16[2048,256]{1,0:T(8,128)(2,1)}, u32[]{:S(2)}) copy-start(bf16[2048,256]{1,0:T(8,128)(2,1)} %param.19) | copy-start | bytes 3145732
  14.5 2.3 %copy-start.4 = (bf16[2048,1280]{1,0:T(8,128)(2,1)}, bf16[2048,1280]{1,0:T(8,128)(2,1)S(1)}, u32[]{:S(2)}) copy-start(bf16[2048,1280]{1,0:T(8,128)(2,1)S(1)} %constant_dynamic-update-slice_fusion) | copy-start | bytes 15728644
  57.8 13.9 %copy-start.5 = (f32[3,256]{1,0:T(4,128)S(1)}, f32[3,256]{1,0:T(4,128)}, u32[]{:S(2)}) copy-start(f32[3,256]{1,0:T(4,128)} %param.20) | copy-start | bytes 9220
  67.1 6.5 %collective-permute-start.1 = (bf16[128,512]{1,0:T(8,128)(2,1)}, bf16[128,512]{1,0:T(8,128)(2,1)}, u32[]{:S(2)}, u32[]{:S(2)}) collective-permute-start(bf16[128,512]{1,0:T(8,128)(2,1)} %get-tuple-element.10), channel_id=1, source_target_pairs={{2,0},{4,2},{6,4},{8,6},{10,8},{12,10},{14,12},{16,14},{18,16},{20... | collective-permute-start | bytes 393224 | tf_op jit(solution)/shard_map/ppermute | solution.py:20
  69.7 7.5 %collective-permute-start = (bf16[128,512]{1,0:T(8,128)(2,1)}, bf16[128,512]{1,0:T(8,128)(2,1)}, u32[]{:S(2)}, u32[]{:S(2)}) collective-permute-start(bf16[128,512]{1,0:T(8,128)(2,1)} %get-tuple-element.9), channel_id=1, source_target_pairs={{0,2},{2,4},{4,6},{6,8},{8,10},{10,12},{12,14},{14,16},{16,18},{18... | collective-permute-start | bytes 393224 | tf_op jit(solution)/shard_map/ppermute | solution.py:17
  81.0 15.0 %all-to-all-start.1 = ((bf16[2,384,256]{1,2,0:T(8,128)(2,1)}), bf16[2,384,256]{1,2,0:T(8,128)(2,1)S(1)}, u32[]{:S(2)}, u32[]{:S(2)}) async-start(bf16[2,384,256]{1,2,0:T(8,128)(2,1)} %copy.21), calls=%async_computation.1 | async-start | bytes 786432 | tf_op jit(solution)/shard_map/all_to_all | solution.py:132
Sparse Core Ops, SparseCore 0:
  11.7 46.0 all-gather.1
where the time goes:
time: 117 us
  waiting for transfers between devices  43.3 us (37%)
  matrix products  19.9 us (17%)
  between operations  13.6 us (12%)
  other arithmetic  12.8 us (11%)
  local copies, waits for them, and re-layouts  10.1 us (9%)
  blocking collectives  8.77 us (7%)
  starting transfers between devices  8.19 us (7%)
    all_gather x1, waiting for transfers between devices, body(): lax.all_gather(normed, 'tp', axis=0, tiled=True)  39.7 us
    all_to_all x1, blocking collectives, body(): lax.all_to_all(attended, 'tp', split_axis=0, concat_axis=1, tiled=True)  8.77 us
    dot_general x1, matrix products, body(): jnp.dot(lax.all_gather(normed, 'tp', axis=0, tiled=True), all_weight, pre...  7.67 us
    dot_general x1, matrix products, body(): jnp.dot(joined, out_weight, preferred_element_type=jnp.float32)  5.15 us
    unnamed x19, local copies, waits for them, and re-layouts  4.92 us
    dot_general x1, matrix products, attend_local(): jnp.einsum('bhcv,vbn->cbhn', weight_lower_precision, value_block_tile, pr...  3.85 us
    all_to_all x1, starting transfers between devices, body(): lax.all_to_all(conv_out, 'tp', split_axis=0, concat_axis=1, tiled=True)  3.65 us
    ppermute x1, waiting for transfers between devices, extended(): lax.ppermute(lax.slice_in_dim(block, block.shape[dim] - width, None, axis...  3.63 us
  transfers between devices with their start and end apart: 4, of which 2 were waited for; matrix products, arithmetic and copies ran while one was open for 15% of the time, Pallas kernels for 0%

commit v1 on v0

--- a/solution.py
+++ b/solution.py
@@ -1,7 +1,12 @@
+import functools
+
 import jax
 import jax.numpy as jnp
 from jax import lax
+from jax.experimental import pallas as pl
+from jax.experimental.pallas import tpu as pltpu
 from jax.sharding import PartitionSpec as P
+
 
 QH = 8
 KVH = 4
@@ -134,6 +139,398 @@
     joined = jnp.concatenate([attn_rows, conv_rows], axis=1)
     return jnp.dot(joined, out_weight, preferred_element_type=jnp.float32).astype(jnp.bfloat16)
 
+EDGE = 16
+ORDER = ("key", "value", "query", "gate", "pre", "input")
+BF16 = jnp.bfloat16
+F32 = jnp.float32
+
+
+def gather_kernel(
+    line,
+    tokens,
+    gain,
+    w_key,
+    w_value,
+    w_query,
+    w_gate,
+    w_pre,
+    w_input,
+    small,
+    q_out,
+    kv_out,
+    gate_out,
+    prod_out,
+    small_out,
+    g_key,
+    g_value,
+    g_query,
+    g_gate,
+    g_pre,
+    g_input,
+    normed,
+    edge_low,
+    edge_high,
+    pre_buf,
+    send_sem,
+    recv_sem,
+    aux_send,
+    aux_recv,
+    local_sem,
+):
+    own = (w_key, w_value, w_query, w_gate, w_pre, w_input)
+    got = (g_key, g_value, g_query, g_gate, g_pre, g_input)
+    count = tokens.shape[0]
+    depth = tokens.shape[1]
+    s = lax.axis_index("sp")
+    t = lax.axis_index("tp")
+    other = 1 - t
+    c = lax.rem(s, 2)
+    y = lax.rem(s // 2, 2)
+    z = s // 4
+    n_sp = 4 * line
+    chunks = n_sp
+    rows = depth // chunks
+    flat = 2 * s + t
+    has_prev, has_next = flat > 0, flat < 2 * n_sp - 1
+    prev = {"sp": jnp.maximum(flat - 1, 0) // 2, "tp": other}
+    nxt = {"sp": jnp.minimum(flat + 1, 2 * n_sp - 1) // 2, "tp": other}
+    has_left, has_right = z > 0, z < line - 1
+    x_dev = {"sp": s, "tp": other}
+    y_dev = {"sp": s + 2 - 4 * y, "tp": t}
+    core_dev = {"sp": s + 1 - 2 * c, "tp": t}
+    left_dev = {"sp": jnp.maximum(s - 4, lax.rem(s, 4)), "tp": t}
+    right_dev = {"sp": jnp.minimum(s + 4, n_sp - 4 + lax.rem(s, 4)), "tp": t}
+
+    def maybe(cond, fn):
+        if cond is None:
+            fn()
+        else:
+            pl.when(cond)(fn)
+
+    barrier = pltpu.get_barrier_semaphore()
+    greet = (
+        (None, x_dev),
+        (None, y_dev),
+        (None, core_dev),
+        (has_left, left_dev),
+        (has_right, right_dev),
+        (has_prev, prev),
+        (has_next, nxt),
+    )
+    for cond, dev in greet:
+        maybe(cond, lambda dev=dev: pl.semaphore_signal(barrier, inc=1, device_id=dev))
+    peers = sum(1 if cond is None else cond.astype(jnp.int32) for cond, _ in greet)
+    pl.semaphore_wait(barrier, peers)
+
+    def chunk_of(core, yy, zz):
+        return (core * 2 + yy) * line + zz
+
+    def piece(ref, ch):
+        return ref.at[pl.ds(pl.multiple_of(ch * rows, rows), rows), :]
+
+    sends = []
+
+    def send(cond, a, ch, dev, slot, first=False):
+        copy = pltpu.make_async_remote_copy(
+            src_ref=piece(own[a] if first else got[a], ch),
+            dst_ref=piece(got[a], ch),
+            send_sem=send_sem.at[a, slot],
+            recv_sem=recv_sem.at[a, ch],
+            device_id=dev,
+        )
+        maybe(cond, copy.start)
+        sends.append((cond, copy))
+
+    def arrived(cond, a, ch):
+        part = piece(got[a], ch)
+        maybe(cond, pltpu.make_async_copy(part, part, recv_sem.at[a, ch]).wait)
+
+    aux = []
+
+    def aux_copy(cond, src, dst, dev, slot, to_slot):
+        copy = pltpu.make_async_remote_copy(
+            src_ref=src,
+            dst_ref=dst,
+            send_sem=aux_send.at[slot],
+            recv_sem=aux_recv.at[to_slot],
+            device_id=dev,
+        )
+        maybe(cond, copy.start)
+        aux.append((cond, copy))
+
+    def aux_wait(cond, dst, slot):
+        maybe(cond, pltpu.make_async_copy(dst, dst, aux_recv.at[slot]).wait)
+
+    X0, X1, ZR, ZL, YS, CS = 0, 1, 2, 2 + line, 2 + 2 * line, 2 + 4 * line
+
+    def x_sends(a):
+        send(None, a, chunk_of(c, y, z), x_dev, X0, first=True)
+        send(None, a, chunk_of(c, 1 - y, z), x_dev, X1, first=True)
+
+    for a in range(2):
+        x_sends(a)
+    aux_copy(has_next, tokens.at[count - EDGE : count, :], edge_low, nxt, 0, 0)
+    aux_copy(has_prev, tokens.at[0:EDGE, :], edge_high, prev, 1, 1)
+    aux_copy(None, small, small_out.at[t], x_dev, 2, 2)
+    for a in range(2, 6):
+        x_sends(a)
+    mine = pltpu.make_async_copy(small, small_out.at[t], local_sem.at[0])
+    mine.start()
+
+    def stage(a, d):
+        if d == 0:
+            arrived(None, a, chunk_of(c, y, z))
+            send(has_right, a, chunk_of(c, y, z), right_dev, ZR)
+            send(has_left, a, chunk_of(c, y, z), left_dev, ZL)
+            send(None, a, chunk_of(c, y, z), core_dev, CS)
+            arrived(None, a, chunk_of(c, 1 - y, z))
+            send(None, a, chunk_of(c, 1 - y, z), core_dev, CS + 1)
+            return
+        if d < line:
+            for side, (zz, here, onward, dev, slot) in enumerate(
+                (
+                    (z - d, z - d >= 0, has_right, right_dev, ZR + d),
+                    (z + d, z + d < line, has_left, left_dev, ZL + d),
+                )
+            ):
+                ch = chunk_of(c, y, jnp.clip(zz, 0, line - 1))
+                arrived(here, a, ch)
+                if d < line - 1:
+                    send(here & onward, a, ch, dev, slot)
+                send(here, a, ch, y_dev, YS + 2 * (d - 1) + side)
+                send(here, a, ch, core_dev, CS + 2 * d + side)
+        if d > 1:
+            for side, (zz, here) in enumerate(((z - d + 1, z - d + 1 >= 0), (z + d - 1, z + d - 1 < line))):
+                ch = chunk_of(c, 1 - y, jnp.clip(zz, 0, line - 1))
+                arrived(here, a, ch)
+                send(here, a, ch, core_dev, CS + 2 * (line + d - 2) + side)
+
+    def complete(a):
+        for i in range(2 * line):
+            arrived(None, a, chunk_of(1 - c, 0, 0) + i)
+
+    def norm(block):
+        f = block.astype(F32)
+        scale = lax.rsqrt(jnp.mean(f * f, axis=-1, keepdims=True) + 1e-06)
+        return (f * scale * gain[...]).astype(BF16)
+
+    def norm_main():
+        def step(i, carry):
+            r = pl.multiple_of(i * EDGE, EDGE)
+            normed[pl.ds(r + EDGE, EDGE), :] = norm(tokens[pl.ds(r, EDGE), :])
+            return carry
+
+        lax.fori_loop(0, count // EDGE, step, 0, unroll=2)
+
+    def norm_edges():
+        aux_wait(has_prev, edge_low, 0)
+        aux_wait(has_next, edge_high, 1)
+
+        @pl.when(jnp.logical_not(has_prev))
+        def _():
+            edge_low[...] = jnp.zeros_like(edge_low)
+
+        @pl.when(jnp.logical_not(has_next))
+        def _():
+            edge_high[...] = jnp.zeros_like(edge_high)
+
+        normed[0:EDGE, :] = norm(edge_low[...])
+        normed[count + EDGE :, :] = norm(edge_high[...])
+
+    def lanes(ref, side, base=0):
+        width = ref.shape[1]
+        return pl.ds(pl.multiple_of(base + side * width, 128), width)
+
+    def project(a, ref, side):
+        kind = ORDER[a]
+        if kind in ("pre", "input"):
+            result = jnp.dot(normed[...], ref[...], preferred_element_type=F32).astype(BF16)
+            if kind == "pre":
+                pre_buf[:, lanes(ref, side)] = result
+            else:
+                cols = lanes(ref, side)
+                prod_out[:, cols] = (
+                    pre_buf[:, cols].astype(F32) * result.astype(F32)
+                ).astype(BF16)
+            return
+        result = jnp.dot(
+            normed[EDGE : EDGE + count, :], ref[...], preferred_element_type=F32
+        ).astype(BF16)
+        if kind == "query":
+            q_out[:, lanes(ref, side)] = result
+        elif kind == "gate":
+            gate_out[:, lanes(ref, side)] = result
+        else:
+            base = 0 if kind == "key" else 2 * w_key.shape[1]
+            kv_out[WIN : WIN + count, lanes(ref, side, base)] = result
+
+    def send_halo():
+        aux_copy(
+            has_next, kv_out.at[count : count + WIN, :], kv_out.at[0:WIN, :], nxt, 3, 3
+        )
+        aux_copy(
+            has_prev,
+            kv_out.at[WIN : 2 * WIN, :],
+            kv_out.at[count + WIN : count + 2 * WIN, :],
+            prev,
+            4,
+            4,
+        )
+
+    norm_main()
+    for wave in range(6 + line + 1):
+        for d in range(line, -1, -1):
+            if 0 <= wave - d < 6:
+                stage(wave - d, d)
+        if wave == 4:
+            norm_edges()
+        if wave < 6:
+            project(wave, own[wave], t)
+        done = wave - line - 1
+        if 0 <= done < 6:
+            complete(done)
+            project(done, got[done], other)
+            if done == 1:
+                send_halo()
+
+    @pl.when(jnp.logical_not(has_prev))
+    def _():
+        kv_out[0:WIN, :] = jnp.zeros((WIN, kv_out.shape[1]), BF16)
+
+    @pl.when(jnp.logical_not(has_next))
+    def _():
+        kv_out[count + WIN :, :] = jnp.zeros((WIN, kv_out.shape[1]), BF16)
+
+    aux_wait(None, small_out.at[other], 2)
+    mine.wait()
+    aux_wait(has_prev, kv_out.at[0:WIN, :], 3)
+    aux_wait(has_next, kv_out.at[count + WIN : count + 2 * WIN, :], 4)
+    for cond, copy in sends + aux:
+        maybe(cond, copy.wait_send)
+
+
+def mix_kernel(total, q_ref, kv_ref, gate_ref, prod_ref, small_ref, weight_ref, out_ref):
+    count, heads_width = q_ref.shape[0], q_ref.shape[1]
+    block = WIN
+    step = pl.program_id(0)
+    span = block + 2 * WIN
+    start = (lax.axis_index("sp") * 2 + lax.axis_index("tp")) * (pl.num_programs(0) * block)
+    start = start + step * block
+    base = pl.multiple_of(step * block, block)
+    row = lax.broadcasted_iota(jnp.int32, (block, span), 0)
+    col = lax.broadcasted_iota(jnp.int32, (block, span), 1)
+    key_pos = start - WIN + col
+    valid = (col >= row) & (col - row <= 2 * WIN) & (key_pos >= 0) & (key_pos < total)
+    kv_width = kv_ref.shape[1] // 2
+    ratio = QH // KVH
+    per_side = QH // 2
+    pieces = []
+    for h in range(QH):
+        g = h // ratio
+        q = q_ref[:, h * HEAD_SIZE : (h + 1) * HEAD_SIZE]
+        k = kv_ref[pl.ds(base, span), g * HEAD_SIZE : (g + 1) * HEAD_SIZE]
+        v = kv_ref[pl.ds(base, span), kv_width + g * HEAD_SIZE : kv_width + (g + 1) * HEAD_SIZE]
+        scores = lax.dot_general(
+            q, k, (((1,), (1,)), ((), ())), preferred_element_type=F32
+        ) * HEAD_SIZE ** (-0.5)
+        scores = jnp.where(valid, scores, -jnp.inf)
+        i = h % per_side
+        sink = small_ref[h // per_side, 3:4, i : i + 1]
+        top = jnp.maximum(jnp.max(scores, axis=-1, keepdims=True), sink)
+        expo = jnp.exp(scores - top)
+        denom = jnp.sum(expo, axis=-1, keepdims=True) + jnp.exp(sink - top)
+        weights = (expo * (1.0 / denom)).astype(BF16)
+        pieces.append(jnp.dot(weights, v, preferred_element_type=F32).astype(BF16))
+    attended = jnp.concatenate(pieces, axis=1)
+    window = prod_ref[pl.ds(base, block + 2 * EDGE), :].astype(F32)
+    taps = [
+        jnp.concatenate([small_ref[0, j : j + 1, :], small_ref[1, j : j + 1, :]], axis=1)
+        for j in range(3)
+    ]
+    convolved = (
+        taps[0] * window[EDGE - 1 : EDGE - 1 + block]
+        + taps[1] * window[EDGE : EDGE + block]
+        + taps[2] * window[EDGE + 1 : EDGE + 1 + block]
+    )
+    conv_out = (gate_ref[...].astype(F32) * convolved).astype(BF16)
+    joined = jnp.concatenate([attended, conv_out], axis=1)
+    out_ref[...] = jnp.dot(joined, weight_ref[...], preferred_element_type=F32).astype(BF16)
+
+
+def fast_body(
+    line,
+    tokens,
+    norm_gain,
+    query_weight,
+    key_weight,
+    value_weight,
+    sink_logit,
+    conv_gate_weight,
+    conv_pre_weight,
+    conv_input_weight,
+    conv_taps,
+    out_weight,
+):
+    count, depth = tokens.shape
+    width = conv_taps.shape[1]
+    small = jnp.concatenate(
+        [
+            conv_taps,
+            jnp.pad(sink_logit[None, :], ((0, 0), (0, width - sink_logit.shape[0]))),
+            jnp.zeros((4, width), F32),
+        ],
+        axis=0,
+    )
+    weights = (
+        key_weight,
+        value_weight,
+        query_weight,
+        conv_gate_weight,
+        conv_pre_weight,
+        conv_input_weight,
+    )
+    vmem = pl.BlockSpec(memory_space=pltpu.VMEM)
+    kv_width = 2 * (key_weight.shape[1] + value_weight.shape[1])
+    extended_rows = count + 2 * EDGE
+    q, kv, gate, prod, small_all = pl.pallas_call(
+        functools.partial(gather_kernel, line),
+        out_shape=(
+            jax.ShapeDtypeStruct((count, 2 * query_weight.shape[1]), BF16),
+            jax.ShapeDtypeStruct((count + 2 * WIN, kv_width), BF16),
+            jax.ShapeDtypeStruct((count, 2 * width), BF16),
+            jax.ShapeDtypeStruct((extended_rows, 2 * width), BF16),
+            jax.ShapeDtypeStruct((2, 8, width), F32),
+        ),
+        in_specs=[vmem] * 9,
+        out_specs=(vmem,) * 5,
+        scratch_shapes=[pltpu.VMEM(w.shape, BF16) for w in weights]
+        + [
+            pltpu.VMEM((extended_rows, depth), BF16),
+            pltpu.VMEM((EDGE, depth), BF16),
+            pltpu.VMEM((EDGE, depth), BF16),
+            pltpu.VMEM((extended_rows, 2 * width), BF16),
+            pltpu.SemaphoreType.DMA((6, 2 + 8 * line)),
+            pltpu.SemaphoreType.DMA((6, 4 * line)),
+            pltpu.SemaphoreType.DMA((5,)),
+            pltpu.SemaphoreType.DMA((5,)),
+            pltpu.SemaphoreType.DMA((1,)),
+        ],
+        compiler_params=pltpu.CompilerParams(
+            collective_id=0, has_side_effects=True, vmem_limit_bytes=40 * 2**20
+        ),
+    )(tokens, norm_gain.reshape(1, depth), *weights, small)
+    blocks = count // WIN
+    whole = lambda a: pl.BlockSpec(a.shape, lambda i: (0,) * a.ndim)
+    tile = lambda a: pl.BlockSpec((WIN, a.shape[1]), lambda i: (i, 0))
+    return pl.pallas_call(
+        functools.partial(mix_kernel, count * 8 * line),
+        grid=(blocks,),
+        out_shape=jax.ShapeDtypeStruct((count, out_weight.shape[1]), BF16),
+        in_specs=[tile(q), whole(kv), tile(gate), whole(prod), whole(small_all), whole(out_weight)],
+        out_specs=pl.BlockSpec((WIN, out_weight.shape[1]), lambda i: (i, 0)),
+        compiler_params=pltpu.CompilerParams(vmem_limit_bytes=40 * 2**20),
+    )(q, kv, gate, prod, small_all, out_weight)
+
 
 def solution(mesh):
     placed = (
@@ -149,6 +546,10 @@
         P(None, "tp"),
         P(),
     )
+    n_sp, n_tp = mesh.shape["sp"], mesh.shape["tp"]
+    line = n_sp // 4
+    paired = n_tp == 2 and n_sp % 4 == 0 and line >= 2
+    chosen = functools.partial(fast_body, line) if paired else body
     return jax.shard_map(
-        body, mesh=mesh, in_specs=placed, out_specs=P(("sp", "tp"), None), check_vma=False
-    )
+        chosen, mesh=mesh, in_specs=placed, out_specs=P(("sp", "tp"), None), check_vma=False
+    )

time: 117 us -> 77.1 us (0.66)
  the two profiles are of different devices: /device:TPU:8 before, /device:TPU:0 now
where the time goes in v1:
time: 77.1 us; the launch traced here: 76.6 us
  Pallas kernels  66.7 us (87%)
  local copies, waits for them, and re-layouts  9.16 us (12%)
    pallas_call x1, Pallas kernels, fast_body(): pl.pallas_call(functools.partial(gather_kernel, line), out_shape=(jax.Sha...  51.1 us
    pallas_call x1, Pallas kernels, fast_body(): pl.pallas_call(functools.partial(mix_kernel, count * 8 * line), grid=(blo...  15.5 us
    unnamed x18, local copies, waits for them, and re-layouts  9.09 us

profile of v1, /device:TPU:0, one launch (start us, length us, event | category | flops | bytes accessed | tf_op | source)
XLA Modules:
  0.0 76.6 jit_solution(13072865985019671049)
XLA Ops:
  0.0 0.1 pad.7.clone
  0.1 0.8 %fusion.small = f32[8,256]{1,0:T(8,128)S(1)} fusion(f32[1,4]{1,0:T(1,128)} %bitcast.3, f32[3,256]{1,0:T(4,128)} %param.20, f32[8]{0:T(128)S(1)} %pad.7.clone), kind=kLoop, calls=%fused_computation.3 | loop fusion | flops 12288 | bytes 11312 | tf_op jit(solution)/shard_map/concatenate | solution.py:476
  0.9 0.0 copy-start.1
  0.9 1.4 %copy-done.1 = bf16[384,2048]{1,0:T(8,128)(2,1)S(1)} copy-done((bf16[384,2048]{1,0:T(8,128)(2,1)S(1)}, bf16[384,2048]{1,0:T(8,128)(2,1)}, u32[]{:S(2)}) %copy-start.1) | copy-done | bytes 1572888
  2.3 0.0 copy-start.2
  2.3 1.2 %copy-done.2 = bf16[2048,256]{1,0:T(8,128)(2,1)S(1)} copy-done((bf16[2048,256]{1,0:T(8,128)(2,1)S(1)}, bf16[2048,256]{1,0:T(8,128)(2,1)}, u32[]{:S(2)}) %copy-start.2) | copy-done | bytes 1048600
  3.5 0.0 copy-start.3
  3.5 1.2 %copy-done.3 = bf16[2048,256]{1,0:T(8,128)(2,1)S(1)} copy-done((bf16[2048,256]{1,0:T(8,128)(2,1)S(1)}, bf16[2048,256]{1,0:T(8,128)(2,1)}, u32[]{:S(2)}) %copy-start.3) | copy-done | bytes 1048600
  4.7 0.0 copy-start.4
  4.7 1.2 %copy-done.4 = bf16[2048,256]{1,0:T(8,128)(2,1)S(1)} copy-done((bf16[2048,256]{1,0:T(8,128)(2,1)S(1)}, bf16[2048,256]{1,0:T(8,128)(2,1)}, u32[]{:S(2)}) %copy-start.4) | copy-done | bytes 1048600
  5.9 0.0 copy-start.5
  5.9 1.2 %copy-done.5 = bf16[2048,256]{1,0:T(8,128)(2,1)S(1)} copy-done((bf16[2048,256]{1,0:T(8,128)(2,1)S(1)}, bf16[2048,256]{1,0:T(8,128)(2,1)}, u32[]{:S(2)}) %copy-start.5) | copy-done | bytes 1048600
  7.2 0.0 copy-start.6
  7.2 1.0 %copy-done.6 = bf16[2048,128]{1,0:T(8,128)(2,1)S(1)} copy-done((bf16[2048,128]{1,0:T(8,128)(2,1)S(1)}, bf16[2048,128]{1,0:T(8,128)(2,1)}, u32[]{:S(2)}) %copy-start.6) | copy-done | bytes 524312
  8.2 0.0 copy-start.7
  8.2 1.0 %copy-done.7 = bf16[2048,128]{1,0:T(8,128)(2,1)S(1)} copy-done((bf16[2048,128]{1,0:T(8,128)(2,1)S(1)}, bf16[2048,128]{1,0:T(8,128)(2,1)}, u32[]{:S(2)}) %copy-start.7) | copy-done | bytes 524312
  9.2 0.0 copy-start.8
  9.2 0.7 copy-done.8
  9.9 0.0 copy-start
  9.9 51.1 %shard_map.109 = (bf16[384,512]{1,0:T(8,128)(2,1)S(1)}, bf16[640,512]{1,0:T(8,128)(2,1)S(1)}, bf16[384,512]{1,0:T(8,128)(2,1)S(1)}, bf16[416,512]{1,0:T(8,128)(2,1)S(1)}, f32[2,8,256]{2,1,0:T(8,128)S(1)}) custom-call(bf16[384,2048]{1,0:T(8,128)(2,1)S(1)} %copy-done.1, f32[1,2048]{1,0:T(1,128)S(1)} %bitcast.2, bf16[2048,128]{1,0:T(8,128)(2,1)S(1)} %copy-done.6, ...), custom_call_target="tpu_custom_call" | custom-call | tf_op jit(solution)/shard_map/pallas_call | solution.py:495
  61.1 0.0 copy-done
  61.1 15.5 %shard_map.110 = bf16[384,2048]{1,0:T(8,128)(2,1)} custom-call(bf16[384,512]{1,0:T(8,128)(2,1)S(1)} %get-tuple-element.10.q_ref, bf16[640,512]{1,0:T(8,128)(2,1)S(1)} %get-tuple-element.11.kv_ref, bf16[384,512]{1,0:T(8,128)(2,1)S(1)} %get-tuple-element.12.gate_ref, bf16[416,512]{1,0:T(8,128)(2,1)S(1)} %get-tuple-element.13.prod_ref, ...), custom_call_target="tpu_custom_call" | custom-call | tf_op jit(solution)/shard_map/pallas_call | solution.py:525
  (1 shorter events, 0.0 us)
Async XLA Ops:
  0.9 1.4 %copy-start.1 = (bf16[384,2048]{1,0:T(8,128)(2,1)S(1)}, bf16[384,2048]{1,0:T(8,128)(2,1)}, u32[]{:S(2)}) copy-start(bf16[384,2048]{1,0:T(8,128)(2,1)} %tokens.1) | copy-start | bytes 4718596
  2.3 1.2 %copy-start.2 = (bf16[2048,256]{1,0:T(8,128)(2,1)S(1)}, bf16[2048,256]{1,0:T(8,128)(2,1)}, u32[]{:S(2)}) copy-start(bf16[2048,256]{1,0:T(8,128)(2,1)} %w_query.1) | copy-start | bytes 3145732
  3.5 1.2 %copy-start.3 = (bf16[2048,256]{1,0:T(8,128)(2,1)S(1)}, bf16[2048,256]{1,0:T(8,128)(2,1)}, u32[]{:S(2)}) copy-start(bf16[2048,256]{1,0:T(8,128)(2,1)} %w_gate.1) | copy-start | bytes 3145732
  4.7 1.2 %copy-start.4 = (bf16[2048,256]{1,0:T(8,128)(2,1)S(1)}, bf16[2048,256]{1,0:T(8,128)(2,1)}, u32[]{:S(2)}) copy-start(bf16[2048,256]{1,0:T(8,128)(2,1)} %w_pre.1) | copy-start | bytes 3145732
  5.9 1.2 %copy-start.5 = (bf16[2048,256]{1,0:T(8,128)(2,1)S(1)}, bf16[2048,256]{1,0:T(8,128)(2,1)}, u32[]{:S(2)}) copy-start(bf16[2048,256]{1,0:T(8,128)(2,1)} %w_input.1) | copy-start | bytes 3145732
  7.2 1.0 %copy-start.6 = (bf16[2048,128]{1,0:T(8,128)(2,1)S(1)}, bf16[2048,128]{1,0:T(8,128)(2,1)}, u32[]{:S(2)}) copy-start(bf16[2048,128]{1,0:T(8,128)(2,1)} %w_key.1) | copy-start | bytes 1572868
  8.2 1.0 %copy-start.7 = (bf16[2048,128]{1,0:T(8,128)(2,1)S(1)}, bf16[2048,128]{1,0:T(8,128)(2,1)}, u32[]{:S(2)}) copy-start(bf16[2048,128]{1,0:T(8,128)(2,1)} %w_value.1) | copy-start | bytes 1572868
  9.2 0.7 copy-start.8
  9.9 51.1 %copy-start = (bf16[1024,2048]{1,0:T(8,128)(2,1)S(1)}, bf16[1024,2048]{1,0:T(8,128)(2,1)}, u32[]{:S(2)}) copy-start(bf16[1024,2048]{1,0:T(8,128)(2,1)} %weight_ref.1) | copy-start | bytes 12582916

commit v2 on v1

--- a/solution.py
+++ b/solution.py
@@ -147,20 +147,32 @@
 
 def gather_kernel(
     line,
+    tokens_hbm,
+    gain,
+    h_key,
+    h_value,
+    h_query,
+    h_gate,
+    h_pre,
+    h_input,
+    small,
+    out_hbm,
+    result_ref,
     tokens,
-    gain,
     w_key,
     w_value,
     w_query,
     w_gate,
     w_pre,
     w_input,
-    small,
+    out_weight,
     q_out,
     kv_out,
     gate_out,
     prod_out,
     small_out,
+    attended,
+    partial,
     g_key,
     g_value,
     g_query,
@@ -177,6 +189,7 @@
     aux_recv,
     local_sem,
 ):
+    held = (h_key, h_value, h_query, h_gate, h_pre, h_input)
     own = (w_key, w_value, w_query, w_gate, w_pre, w_input)
     got = (g_key, g_value, g_query, g_gate, g_pre, g_input)
     count = tokens.shape[0]
@@ -207,6 +220,11 @@
         else:
             pl.when(cond)(fn)
 
+    load_tokens = pltpu.make_async_copy(tokens_hbm, tokens, local_sem.at[1])
+    load_tokens.start()
+    load_out = pltpu.make_async_copy(out_hbm, out_weight, local_sem.at[2])
+    loads = [pltpu.make_async_copy(held[a], own[a], local_sem.at[3 + a]) for a in range(6)]
+
     barrier = pltpu.get_barrier_semaphore()
     greet = (
         (None, x_dev),
@@ -232,7 +250,7 @@
 
     def send(cond, a, ch, dev, slot, first=False):
         copy = pltpu.make_async_remote_copy(
-            src_ref=piece(own[a] if first else got[a], ch),
+            src_ref=piece(held[a] if first else got[a], ch),
             dst_ref=piece(got[a], ch),
             send_sem=send_sem.at[a, slot],
             recv_sem=recv_sem.at[a, ch],
@@ -269,8 +287,8 @@
 
     for a in range(2):
         x_sends(a)
-    aux_copy(has_next, tokens.at[count - EDGE : count, :], edge_low, nxt, 0, 0)
-    aux_copy(has_prev, tokens.at[0:EDGE, :], edge_high, prev, 1, 1)
+    aux_copy(has_next, tokens_hbm.at[count - EDGE : count, :], edge_low, nxt, 0, 0)
+    aux_copy(has_prev, tokens_hbm.at[0:EDGE, :], edge_high, prev, 1, 1)
     aux_copy(None, small, small_out.at[t], x_dev, 2, 2)
     for a in range(2, 6):
         x_sends(a)
@@ -377,84 +395,119 @@
             4,
         )
 
+    def attend(b):
+        span = 3 * WIN
+        base = b * WIN
+        row = lax.broadcasted_iota(jnp.int32, (WIN, span), 0)
+        col = lax.broadcasted_iota(jnp.int32, (WIN, span), 1)
+        key_pos = flat * count + base - WIN + col
+        valid = (
+            (col >= row)
+            & (col - row <= 2 * WIN)
+            & (key_pos >= 0)
+            & (key_pos < 2 * n_sp * count)
+        )
+        kv_width = kv_out.shape[1] // 2
+        ratio = QH // KVH
+        per_side = QH // 2
+        for g in range(KVH):
+            k = kv_out[base : base + span, g * HEAD_SIZE : (g + 1) * HEAD_SIZE]
+            v = kv_out[
+                base : base + span,
+                kv_width + g * HEAD_SIZE : kv_width + (g + 1) * HEAD_SIZE,
+            ]
+            parts = []
+            for h in range(g * ratio, (g + 1) * ratio):
+                q = q_out[base : base + WIN, h * HEAD_SIZE : (h + 1) * HEAD_SIZE]
+                scores = lax.dot_general(
+                    q, k, (((1,), (1,)), ((), ())), preferred_element_type=F32
+                ) * HEAD_SIZE ** (-0.5)
+                scores = jnp.where(valid, scores, -jnp.inf)
+                i = h % per_side
+                sink = small_out[h // per_side, 3:4, i : i + 1]
+                top = jnp.maximum(jnp.max(scores, axis=-1, keepdims=True), sink)
+                expo = jnp.exp(scores - top)
+                denom = jnp.sum(expo, axis=-1, keepdims=True) + jnp.exp(sink - top)
+                weights = (expo * (1.0 / denom)).astype(BF16)
+                parts.append(jnp.dot(weights, v, preferred_element_type=F32).astype(BF16))
+            width = ratio * HEAD_SIZE
+            attended[base : base + WIN, g * width : (g + 1) * width] = jnp.concatenate(
+                parts, axis=1
+            )
+
+    def before_attention():
+        @pl.when(jnp.logical_not(has_prev))
+        def _():
+            kv_out[0:WIN, :] = jnp.zeros((WIN, kv_out.shape[1]), BF16)
+
+        @pl.when(jnp.logical_not(has_next))
+        def _():
+            kv_out[count + WIN :, :] = jnp.zeros((WIN, kv_out.shape[1]), BF16)
+
+        aux_wait(None, small_out.at[other], 2)
+        mine.wait()
+        aux_wait(has_prev, kv_out.at[0:WIN, :], 3)
+        aux_wait(has_next, kv_out.at[count + WIN : count + 2 * WIN, :], 4)
+
+    def finish():
+        half = attended.shape[1]
+        taps = [
+            jnp.concatenate([small_out[0, j : j + 1, :], small_out[1, j : j + 1, :]], axis=1)
+            for j in range(3)
+        ]
+        for b in range(count // WIN):
+            base = b * WIN
+            window = prod_out[base : base + WIN + 2 * EDGE, :].astype(F32)
+            convolved = (
+                taps[0] * window[EDGE - 1 : EDGE - 1 + WIN]
+                + taps[1] * window[EDGE : EDGE + WIN]
+                + taps[2] * window[EDGE + 1 : EDGE + 1 + WIN]
+            )
+            conv_out = (gate_out[base : base + WIN, :].astype(F32) * convolved).astype(BF16)
+            result_ref[base : base + WIN, :] = (
+                partial[base : base + WIN, :]
+                + jnp.dot(conv_out, out_weight[half:, :], preferred_element_type=F32)
+            ).astype(BF16)
+
+    for load in loads:
+        load.start()
+    load_out.start()
+    load_tokens.wait()
     norm_main()
-    for wave in range(6 + line + 1):
+    lag = 2
+    blocks = count // WIN
+    last = 5 + lag * line
+    for wave in range(last + 1):
         for d in range(line, -1, -1):
-            if 0 <= wave - d < 6:
-                stage(wave - d, d)
+            if 0 <= wave - lag * d < 6:
+                stage(wave - lag * d, d)
         if wave == 4:
             norm_edges()
         if wave < 6:
+            loads[wave].wait()
             project(wave, own[wave], t)
-        done = wave - line - 1
+        done = wave - lag * line
         if 0 <= done < 6:
+            if done == 3:
+                before_attention()
+                attend(0)
+            if done == 4:
+                for b in range(1, blocks):
+                    attend(b)
+            if done == 5:
+                load_out.wait()
+                partial[...] = jnp.dot(
+                    attended[...],
+                    out_weight[: attended.shape[1], :],
+                    preferred_element_type=F32,
+                )
             complete(done)
             project(done, got[done], other)
             if done == 1:
                 send_halo()
-
-    @pl.when(jnp.logical_not(has_prev))
-    def _():
-        kv_out[0:WIN, :] = jnp.zeros((WIN, kv_out.shape[1]), BF16)
-
-    @pl.when(jnp.logical_not(has_next))
-    def _():
-        kv_out[count + WIN :, :] = jnp.zeros((WIN, kv_out.shape[1]), BF16)
-
-    aux_wait(None, small_out.at[other], 2)
-    mine.wait()
-    aux_wait(has_prev, kv_out.at[0:WIN, :], 3)
-    aux_wait(has_next, kv_out.at[count + WIN : count + 2 * WIN, :], 4)
+    finish()
     for cond, copy in sends + aux:
         maybe(cond, copy.wait_send)
-
-
-def mix_kernel(total, q_ref, kv_ref, gate_ref, prod_ref, small_ref, weight_ref, out_ref):
-    count, heads_width = q_ref.shape[0], q_ref.shape[1]
-    block = WIN
-    step = pl.program_id(0)
-    span = block + 2 * WIN
-    start = (lax.axis_index("sp") * 2 + lax.axis_index("tp")) * (pl.num_programs(0) * block)
-    start = start + step * block
-    base = pl.multiple_of(step * block, block)
-    row = lax.broadcasted_iota(jnp.int32, (block, span), 0)
-    col = lax.broadcasted_iota(jnp.int32, (block, span), 1)
-    key_pos = start - WIN + col
-    valid = (col >= row) & (col - row <= 2 * WIN) & (key_pos >= 0) & (key_pos < total)
-    kv_width = kv_ref.shape[1] // 2
-    ratio = QH // KVH
-    per_side = QH // 2
-    pieces = []
-    for h in range(QH):
-        g = h // ratio
-        q = q_ref[:, h * HEAD_SIZE : (h + 1) * HEAD_SIZE]
-        k = kv_ref[pl.ds(base, span), g * HEAD_SIZE : (g + 1) * HEAD_SIZE]
-        v = kv_ref[pl.ds(base, span), kv_width + g * HEAD_SIZE : kv_width + (g + 1) * HEAD_SIZE]
-        scores = lax.dot_general(
-            q, k, (((1,), (1,)), ((), ())), preferred_element_type=F32
-        ) * HEAD_SIZE ** (-0.5)
-        scores = jnp.where(valid, scores, -jnp.inf)
-        i = h % per_side
-        sink = small_ref[h // per_side, 3:4, i : i + 1]
-        top = jnp.maximum(jnp.max(scores, axis=-1, keepdims=True), sink)
-        expo = jnp.exp(scores - top)
-        denom = jnp.sum(expo, axis=-1, keepdims=True) + jnp.exp(sink - top)
-        weights = (expo * (1.0 / denom)).astype(BF16)
-        pieces.append(jnp.dot(weights, v, preferred_element_type=F32).astype(BF16))
-    attended = jnp.concatenate(pieces, axis=1)
-    window = prod_ref[pl.ds(base, block + 2 * EDGE), :].astype(F32)
-    taps = [
-        jnp.concatenate([small_ref[0, j : j + 1, :], small_ref[1, j : j + 1, :]], axis=1)
-        for j in range(3)
-    ]
-    convolved = (
-        taps[0] * window[EDGE - 1 : EDGE - 1 + block]
-        + taps[1] * window[EDGE : EDGE + block]
-        + taps[2] * window[EDGE + 1 : EDGE + 1 + block]
-    )
-    conv_out = (gate_ref[...].astype(F32) * convolved).astype(BF16)
-    joined = jnp.concatenate([attended, conv_out], axis=1)
-    out_ref[...] = jnp.dot(joined, weight_ref[...], preferred_element_type=F32).astype(BF16)
 
 
 def fast_body(
@@ -490,20 +543,28 @@
         conv_input_weight,
     )
     vmem = pl.BlockSpec(memory_space=pltpu.VMEM)
+    hbm = pl.BlockSpec(memory_space=pltpu.HBM)
     kv_width = 2 * (key_weight.shape[1] + value_weight.shape[1])
+    heads_width = 2 * query_weight.shape[1]
     extended_rows = count + 2 * EDGE
-    q, kv, gate, prod, small_all = pl.pallas_call(
+    return pl.pallas_call(
         functools.partial(gather_kernel, line),
-        out_shape=(
-            jax.ShapeDtypeStruct((count, 2 * query_weight.shape[1]), BF16),
-            jax.ShapeDtypeStruct((count + 2 * WIN, kv_width), BF16),
-            jax.ShapeDtypeStruct((count, 2 * width), BF16),
-            jax.ShapeDtypeStruct((extended_rows, 2 * width), BF16),
-            jax.ShapeDtypeStruct((2, 8, width), F32),
-        ),
-        in_specs=[vmem] * 9,
-        out_specs=(vmem,) * 5,
-        scratch_shapes=[pltpu.VMEM(w.shape, BF16) for w in weights]
+        out_shape=jax.ShapeDtypeStruct((count, out_weight.shape[1]), BF16),
+        in_specs=[hbm, vmem] + [hbm] * 6 + [vmem, hbm],
+        out_specs=vmem,
+        scratch_shapes=[pltpu.VMEM((count, depth), BF16)]
+        + [pltpu.VMEM(w.shape, BF16) for w in weights]
+        + [
+            pltpu.VMEM(out_weight.shape, BF16),
+            pltpu.VMEM((count, heads_width), BF16),
+            pltpu.VMEM((count + 2 * WIN, kv_width), BF16),
+            pltpu.VMEM((count, 2 * width), BF16),
+            pltpu.VMEM((extended_rows, 2 * width), BF16),
+            pltpu.VMEM((2, 8, width), F32),
+            pltpu.VMEM((count, heads_width), BF16),
+            pltpu.VMEM((count, out_weight.shape[1]), F32),
+        ]
+        + [pltpu.VMEM(w.shape, BF16) for w in weights]
         + [
             pltpu.VMEM((extended_rows, depth), BF16),
             pltpu.VMEM((EDGE, depth), BF16),
@@ -513,23 +574,12 @@
             pltpu.SemaphoreType.DMA((6, 4 * line)),
             pltpu.SemaphoreType.DMA((5,)),
             pltpu.SemaphoreType.DMA((5,)),
-            pltpu.SemaphoreType.DMA((1,)),
+            pltpu.SemaphoreType.DMA((9,)),
         ],
         compiler_params=pltpu.CompilerParams(
-            collective_id=0, has_side_effects=True, vmem_limit_bytes=40 * 2**20
+            collective_id=0, has_side_effects=True, vmem_limit_bytes=58 * 2**20
         ),
-    )(tokens, norm_gain.reshape(1, depth), *weights, small)
-    blocks = count // WIN
-    whole = lambda a: pl.BlockSpec(a.shape, lambda i: (0,) * a.ndim)
-    tile = lambda a: pl.BlockSpec((WIN, a.shape[1]), lambda i: (i, 0))
-    return pl.pallas_call(
-        functools.partial(mix_kernel, count * 8 * line),
-        grid=(blocks,),
-        out_shape=jax.ShapeDtypeStruct((count, out_weight.shape[1]), BF16),
-        in_specs=[tile(q), whole(kv), tile(gate), whole(prod), whole(small_all), whole(out_weight)],
-        out_specs=pl.BlockSpec((WIN, out_weight.shape[1]), lambda i: (i, 0)),
-        compiler_params=pltpu.CompilerParams(vmem_limit_bytes=40 * 2**20),
-    )(q, kv, gate, prod, small_all, out_weight)
+    )(tokens, norm_gain.reshape(1, depth), *weights, small, out_weight)
 
 
 def solution(mesh):

time: 77.1 us -> 70.5 us (0.914)
  the two profiles are of different devices: /device:TPU:0 before, /device:TPU:8 now
where the time goes in v2:
time: 70.5 us; the launch traced here: 69.2 us
  Pallas kernels  65 us (92%)
  local copies, waits for them, and re-layouts  2.81 us (4%)
  other arithmetic  1.37 us (2%)
    pallas_call x1, Pallas kernels, fast_body(): pl.pallas_call(functools.partial(gather_kernel, line), out_shape=jax.Shap...  65 us
    unnamed x1, local copies, waits for them, and re-layouts  2.73 us

profile of v2, /device:TPU:8, one launch (start us, length us, event | category | flops | bytes accessed | tf_op | source)
XLA Modules:
  0.0 69.2 jit_solution(15040190591991777943)
XLA Ops:
  0.0 0.1 pad.7.clone
  0.1 1.4 %fusion.small = f32[8,256]{1,0:T(8,128)} fusion(f32[1,4]{1,0:T(1,128)} %bitcast.3, f32[3,256]{1,0:T(4,128)} %param.20, f32[8]{0:T(128)S(1)} %pad.7.clone), kind=kLoop, calls=%fused_computation.3 | loop fusion | flops 12288 | bytes 11312 | tf_op jit(solution)/shard_map/concatenate | solution.py:529
  1.5 65.0 %shard_map.109 = bf16[384,2048]{1,0:T(8,128)(2,1)} custom-call(bf16[384,2048]{1,0:T(8,128)(2,1)} %tokens_hbm.1, f32[1,2048]{1,0:T(1,128)} %bitcast.2, bf16[2048,128]{1,0:T(8,128)(2,1)} %h_key.1, bf16[2048,128]{1,0:T(8,128)(2,1)} %h_value.1, bf16[2048,256]{1,0:T(8,128)(2,1)} %h_query.1, bf16[2048,256]{1,0:T(8,128)(2,1)} %h_gate.1, bf16[2048,256]{1,0:T(8,128)(2,1)} %h_pre.1, ...), custom_call_target="tpu_custom_call" | custom-call | tf_op jit(solution)/shard_map/pallas_call | solution.py:550
  66.5 2.7 %copy.13 = bf16[384,2048]{1,0:T(8,128)(2,1)} copy(bf16[384,2048]{1,0:T(8,128)(2,1)} %shard_map.109) | data formatting | bytes 3145728
  (1 shorter events, 0.0 us)
